TPU v7x, 32 devices: a whole 2x2x4 slice. The times are simulated.
32 devices in a mesh: sp: 8 (over z, x), tp: 4 (over y, core).
Axes of the slice: x: 2, y: 2, z: 4, core: 2. Of those that a mesh axis runs over, the one named last changes fastest.
Arguments:
- layer_input: bfloat16 [8, 1536, 2048], P('sp', 'tp'), may hold values from -6 to 6
- input_gain: float32 [2048], replicated, may hold values from 0.1 to 1.9
- key_weight: bfloat16 [2048, 512], P('sp', 'tp'), may hold values from -0.125 to 0.125
- value_weight: bfloat16 [2048, 512], P('sp', 'tp'), may hold values from -0.125 to 0.125
- key_gain: float32 [128], replicated, may hold values from 0.1 to 1.9
- stop_shift: bfloat16 [8, 4, 1536], P('sp', None, 'tp'), may hold values from -20 to 0
- new_query: bfloat16 [8, 16, 128], P('sp', 'tp'), may hold values from -6 to 6
- query_gain: float32 [128], replicated, may hold values from 0.1 to 1.9
- out_gain: float32 [128], replicated, may hold values from 0.1 to 1.9
Outputs:
- key_cache: bfloat16 [8, 4, 1536, 128], P('sp', 'tp')
- value_cache: bfloat16 [8, 4, 1536, 128], P('sp', 'tp')
- shift_cache: bfloat16 [8, 4, 1536], P('sp', 'tp')
- first_read: bfloat16 [8, 16, 128], P('sp', 'tp')
All inputs are finite; a program needn't handle non-finite values.
Results may differ from a plain program's by a relative error of at most 0.013.
Values may be sent and summed in bfloat16 or wider, within the bound.
A program may use at most 64 MiB of HBM per device.

v0:
```python
import jax
import jax.numpy as jnp
from jax import lax
from jax.sharding import PartitionSpec as P

KVH = 4
epsilon = 1e-06


def row_norm(value_entries, scaling):
    return (
        value_entries
        * lax.rsqrt(jnp.mean(value_entries * value_entries, axis=-1, keepdims=True) + epsilon)
        * scaling
    )


def shards(
    layer_input,
    input_gain,
    key_weight,
    value_weight,
    key_gain,
    stop_shift,
    new_query,
    query_gain,
    out_gain,
):
    groups = lax.axis_size("tp")
    copies = groups // KVH
    row_count = layer_input.shape[1]
    head_size = new_query.shape[2]
    score_scale = 1.0 / head_size**0.5
    normed = row_norm(layer_input[0].astype(jnp.float32), input_gain).astype(jnp.bfloat16)
    stacked = jnp.stack((key_weight, value_weight), 0)
    full_depth = lax.all_gather(stacked, "sp", axis=1, tiled=True)
    projected = jnp.einsum(
        "rd,kdc->krc",
        normed,
        lax.all_gather(full_depth, "tp", axis=2, tiled=True),
        preferred_element_type=jnp.float32,
    )
    key_rows = row_norm(projected[0].reshape(row_count, KVH, head_size), key_gain).astype(
        jnp.bfloat16
    )
    value_rows = projected[1].reshape(row_count, KVH, head_size).astype(jnp.bfloat16)
    local_shift = stop_shift[0]
    key_slots = jnp.repeat(key_rows, copies, axis=1)
    value_slots = jnp.repeat(value_rows, copies, axis=1)
    shift_slots = jnp.repeat(local_shift.T, copies, axis=1)
    key_got, value_got, shift_got = (
        lax.all_to_all(key_slots, "tp", split_axis=1, concat_axis=0, tiled=True),
        lax.all_to_all(value_slots, "tp", split_axis=1, concat_axis=0, tiled=True),
        lax.all_to_all(shift_slots, "tp", split_axis=1, concat_axis=0, tiled=True),
    )
    key_line = key_got[:, 0, :]
    value_line = value_got[:, 0, :]
    shift_line = shift_got[:, 0]
    length = key_line.shape[0]
    query_rows = row_norm(new_query[0].astype(jnp.float32), query_gain).astype(jnp.bfloat16)
    scores = (
        jnp.einsum("qd,ld->ql", query_rows, key_line, preferred_element_type=jnp.float32)
        * score_scale
    )
    scores = scores + shift_line.astype(jnp.float32)[None, :]
    log_keep = jax.nn.log_sigmoid(-scores)
    inside = lax.cumsum(log_keep, axis=1, reverse=True) - log_keep
    weights = jnp.exp(jax.nn.log_sigmoid(scores) + inside).astype(jnp.bfloat16)
    read_sum = jnp.dot(weights, value_line, preferred_element_type=jnp.float32)
    first_out = row_norm(read_sum, out_gain).astype(jnp.bfloat16)
    return (
        key_line.reshape(1, 1, length, head_size),
        value_line.reshape(1, 1, length, head_size),
        shift_line.reshape(1, 1, length),
        first_out[None],
    )


def solution(mesh):
    placed = (
        P("sp", "tp", None),
        P(),
        P("sp", "tp"),
        P("sp", "tp"),
        P(),
        P("sp", None, "tp"),
        P("sp", "tp", None),
        P(),
        P(),
    )
    return jax.shard_map(
        shards,
        mesh=mesh,
        in_specs=placed,
        out_specs=(
            P("sp", "tp", None, None),
            P("sp", "tp", None, None),
            P("sp", "tp", None),
            P("sp", "tp", None),
        ),
        check_vma=False,
    )
```

profile of v0, /device:TPU:0, one launch (start us, length us, event | category | flops | bytes accessed | tf_op | source)
XLA Modules:
  0.0 125.1 jit_solution(7521093562815016131)
XLA Ops:
  7.2 1.0 copy.25
  8.3 0.9 copy.26
  9.2 0.7 pad_maximum_fusion
  10.0 42.8 %all-gather.3.cloned.1.call-done = bf16[2,2048,128]{1,2,0:T(8,128)(2,1)} async-done(((bf16[2,256,128]{1,2,0:T(8,128)(2,1)}), bf16[2,2048,128]{1,2,0:T(8,128)(2,1)}) %all-gather.3.cloned.1.call-update) | async-done | bytes 1048592 | tf_op jit(solution)/shard_map/all_gather | solution.py:36
  52.8 0.7 copy.36
  53.5 0.5 broadcast.75
  54.0 0.7 reduce.5
  54.7 0.7 reshape.96
  55.3 3.2 %all-to-all-start.2 = ((bf16[4,2,192]{2,1,0:T(2,128)(2,1)}), bf16[4,2,192]{2,1,0:T(2,128)(2,1)S(1)}, u32[]{:S(2)}, u32[]{:S(2)}) async-start(bf16[4,2,192]{2,1,0:T(2,128)(2,1)} %reshape.96), calls=%async_computation.2 | async-start | bytes 8192 | tf_op jit(solution)/shard_map/all_to_all | solution.py:54
  58.6 0.8 fusion.22
  59.4 1.9 %fusion = f32[384]{0:T(512)S(1)} fusion(bf16[1,384,2048]{2,1,0:T(8,128)(2,1)} %param.9), kind=kLoop, calls=%fused_computation.2 | loop fusion | flops 2358912 | bytes 1574400 | tf_op jit(solution)/shard_map/reduce_sum | solution.py:13
  61.4 26.5 %all-gather.5.cloned.1.call-done = bf16[2,2048,512]{1,2,0:T(8,128)(2,1)} async-done(((bf16[2,2048,128]{1,2,0:T(8,128)(2,1)}), bf16[2,2048,512]{1,2,0:T(8,128)(2,1)}) %all-gather.5.cloned.1.call-update) | async-done | bytes 4194320 | tf_op jit(solution)/shard_map/all_gather | solution.py:40
  87.8 4.6 %fusion.10 = f32[2,384,512]{1,2,0:T(8,128)S(1)} fusion(bf16[2,2048,512]{1,2,0:T(8,128)(2,1)} %all-gather.5.cloned.1.call-done, bf16[1,384,2048]{2,1,0:T(8,128)(2,1)S(1)} %copy-done, f32[2048]{0:T(1024)S(1)} %copy-done.6, f32[384]{0:T(512)S(1)} %add_rsqrt_fusion.1), kind=kOutput, calls=%fused_computation.12 | convolution fusion | flops 1613758464 | bytes 7349760 | tf_op jit(solution)/shard_map/rd,kdc->krc/dot_general | solution.py:37
  93.1 1.0 multiply_convert_fusion
  94.1 3.5 %all-to-all-start = ((bf16[384,4,128]{2,0,1:T(8,128)(2,1)}), bf16[384,4,128]{2,0,1:T(8,128)(2,1)S(1)}, u32[]{:S(2)}, u32[]{:S(2)}) async-start(bf16[384,4,128]{2,0,1:T(8,128)(2,1)} %multiply_convert_fusion), calls=%async_computation | async-start | bytes 786432 | tf_op jit(solution)/shard_map/all_to_all | solution.py:52
  97.8 0.9 copy.28
  98.7 6.3 %all-to-all-done = bf16[384,4,128]{2,0,1:T(8,128)(2,1)S(1)} async-done(((bf16[384,4,128]{2,0,1:T(8,128)(2,1)}), bf16[384,4,128]{2,0,1:T(8,128)(2,1)S(1)}, u32[]{:S(2)}, u32[]{:S(2)}) %all-to-all-start) | async-done | bytes 393248 | tf_op jit(solution)/shard_map/all_to_all | solution.py:52
  105.0 3.5 %all-to-all-start.1 = ((bf16[384,4,128]{2,0,1:T(8,128)(2,1)}), bf16[384,4,128]{2,0,1:T(8,128)(2,1)S(1)}, u32[]{:S(2)}, u32[]{:S(2)}) async-start(bf16[384,4,128]{2,0,1:T(8,128)(2,1)} %copy.28), calls=%async_computation.1 | async-start | bytes 786432 | tf_op jit(solution)/shard_map/all_to_all | solution.py:53
  108.8 5.0 %reduce-window.6 = f32[4,12,128]{2,1,0:T(8,128)S(1)} reduce-window(f32[4,12,128]{2,1,0:T(8,128)S(1)} %reshape.89, f32[]{:T(128)} %constant.8.clone.1), window={size=1x1x128 pad=0_0x0_0x0_127}, to_apply=%region_3.4 | reduce-window | flops 780288 | bytes 49156 | tf_op jit(solution)/shard_map/reduce-window
  114.2 1.6 %all-to-all-done.1 = bf16[384,4,128]{2,0,1:T(8,128)(2,1)S(1)} async-done(((bf16[384,4,128]{2,0,1:T(8,128)(2,1)}), bf16[384,4,128]{2,0,1:T(8,128)(2,1)S(1)}, u32[]{:S(2)}, u32[]{:S(2)}) %all-to-all-start.1) | async-done | bytes 393248 | tf_op jit(solution)/shard_map/all_to_all | solution.py:53
  115.8 0.3 multiply_reduce_fusion.1
  116.2 0.6 fusion.25
  116.8 0.7 copy.39
  117.5 0.7 copy.40
  (36 shorter events, 1.6 us)
Async XLA Ops:
  7.2 80.7 %copy-start = (bf16[1,384,2048]{2,1,0:T(8,128)(2,1)S(1)}, bf16[1,384,2048]{2,1,0:T(8,128)(2,1)}, u32[]{:S(2)}) copy-start(bf16[1,384,2048]{2,1,0:T(8,128)(2,1)} %param.9) | copy-start | bytes 4718596
  7.2 80.7 %copy-start.6 = (f32[2048]{0:T(1024)S(1)}, f32[2048]{0:T(1024)}, u32[]{:S(2)}) copy-start(f32[2048]{0:T(1024)} %param.10) | copy-start | bytes 24580
  7.2 45.6 %all-gather.3.cloned.1.call-start = ((), (), s32[]{:S(2)}) async-start(), calls=%async_computation.3 | async-start | bytes 1179648 | tf_op jit(solution)/shard_map/all_gather | solution.py:36
  9.9 77.9 %all-gather.5.cloned.1.call-start = ((), (), s32[]{:S(2)}) async-start(), calls=%async_computation.4 | async-start | bytes 5242880 | tf_op jit(solution)/shard_map/all_gather | solution.py:40
  55.3 38.8 %all-to-all-start.2 = ((bf16[4,2,192]{2,1,0:T(2,128)(2,1)}), bf16[4,2,192]{2,1,0:T(2,128)(2,1)S(1)}, u32[]{:S(2)}, u32[]{:S(2)}) async-start(bf16[4,2,192]{2,1,0:T(2,128)(2,1)} %reshape.96), calls=%async_computation.2 | async-start | bytes 8192 | tf_op jit(solution)/shard_map/all_to_all | solution.py:54
  92.5 0.7 copy-start.3
  92.5 15.9 %copy-start.2 = (bf16[1,4,128]{2,1,0:T(4,128)(2,1)S(1)}, bf16[1,4,128]{2,1,0:T(4,128)(2,1)}, u32[]{:S(2)}) copy-start(bf16[1,4,128]{2,1,0:T(4,128)(2,1)} %param.15) | copy-start | bytes 3076
  92.5 15.9 %copy-start.4 = (f32[128]{0:T(128)S(1)}, f32[128]{0:T(128)}, u32[]{:S(2)}) copy-start(f32[128]{0:T(128)} %param.16) | copy-start | bytes 1540
  92.8 23.3 %copy-start.5 = (f32[128]{0:T(128)S(1)}, f32[128]{0:T(128)}, u32[]{:S(2)}) copy-start(f32[128]{0:T(128)} %param.17) | copy-start | bytes 1540
  94.1 10.8 %all-to-all-start = ((bf16[384,4,128]{2,0,1:T(8,128)(2,1)}), bf16[384,4,128]{2,0,1:T(8,128)(2,1)S(1)}, u32[]{:S(2)}, u32[]{:S(2)}) async-start(bf16[384,4,128]{2,0,1:T(8,128)(2,1)} %multiply_convert_fusion), calls=%async_computation | async-start | bytes 786432 | tf_op jit(solution)/shard_map/all_to_all | solution.py:52
  97.7 20.6 %copy-start.1 = (bf16[4,1,384]{2,1,0:T(2,128)(2,1)}, bf16[4,1,384]{2,1,0:T(2,128)(2,1)S(1)}, u32[]{:S(2)}) copy-start(bf16[4,1,384]{2,1,0:T(2,128)(2,1)S(1)} %reshape.97) | copy-start | bytes 9220
  105.0 10.8 %all-to-all-start.1 = ((bf16[384,4,128]{2,0,1:T(8,128)(2,1)}), bf16[384,4,128]{2,0,1:T(8,128)(2,1)S(1)}, u32[]{:S(2)}, u32[]{:S(2)}) async-start(bf16[384,4,128]{2,0,1:T(8,128)(2,1)} %copy.28), calls=%async_computation.1 | async-start | bytes 786432 | tf_op jit(solution)/shard_map/all_to_all | solution.py:53
Sparse Core Ops, SparseCore 0:
  10.6 42.1 all-gather.2
  54.3 33.4 all-gather.4
where the time goes:
time: 126 us; the launch traced here: 125 us
  waiting for transfers between devices  77.2 us (61%)
  between operations  14.2 us (11%)
  other arithmetic  11.1 us (9%)
  starting transfers between devices  10.2 us (8%)
  local copies, waits for them, and re-layouts  7.15 us (6%)
  matrix products  5.2 us (4%)
    all_gather x1, waiting for transfers between devices, shards(): full_depth = lax.all_gather(stacked, 'sp', axis=1, tiled=True)  42.8 us
    all_gather x1, waiting for transfers between devices, shards(): lax.all_gather(full_depth, 'tp', axis=2, tiled=True)  26.5 us
    all_to_all x1, waiting for transfers between devices, shards(): lax.all_to_all(key_slots, 'tp', split_axis=1, concat_axis=0, tiled=True)  6.25 us
    another operation x2, other arithmetic  5.17 us
    unnamed x21, local copies, waits for them, and re-layouts  4.98 us
    dot_general x1, matrix products, shards(): jnp.einsum('rd,kdc->krc', normed, lax.all_gather(full_depth, 'tp', axis=2...  4.62 us
    all_to_all x1, starting transfers between devices, shards(): lax.all_to_all(key_slots, 'tp', split_axis=1, concat_axis=0, tiled=True)  3.46 us
    all_to_all x1, starting transfers between devices, shards(): lax.all_to_all(value_slots, 'tp', split_axis=1, concat_axis=0, tiled=True)  3.46 us
  transfers between devices with their start and end apart: 5, of which 4 were waited for; matrix products, arithmetic and copies ran while one was open for 14% of the time, Pallas kernels for 0%

commit v1 on v0

--- a/solution.py
+++ b/solution.py
@@ -33,7 +33,12 @@
     score_scale = 1.0 / head_size**0.5
     normed = row_norm(layer_input[0].astype(jnp.float32), input_gain).astype(jnp.bfloat16)
     stacked = jnp.stack((key_weight, value_weight), 0)
-    full_depth = lax.all_gather(stacked, "sp", axis=1, tiled=True)
+    ring = [stacked]
+    for hop in range(7):
+        ring.append(lax.ppermute(ring[-1], "sp", [(dev, (dev + 1) % 8) for dev in range(8)]))
+    full_depth = jnp.roll(
+        jnp.concatenate(ring[::-1], axis=1), (lax.axis_index("sp") + 1) * ring[0].shape[1], axis=1
+    )
     projected = jnp.einsum(
         "rd,kdc->krc",
         normed,

time: 126 us -> 138 us (1.095)
  waiting for transfers between devices: 77.2 us -> 88.3 us
  starting transfers between devices: 10.2 us -> 13.4 us
  other arithmetic: 11.1 us -> 8.25 us
    ppermute x0 -> x7, waiting for transfers between devices: none -> 53.7 us  [shards(): lax.ppermute(ring[-1], 'sp', [(dev, (dev + 1) % 8) for dev in range(8)])]
    all_gather x1 -> x0, waiting for transfers between devices: 42.8 us -> none  [shards(): full_depth = lax.all_gather(stacked, 'sp', axis=1, tiled=True)]
    ppermute x0 -> x7, starting transfers between devices: none -> 3.04 us  [shards(): lax.ppermute(ring[-1], 'sp', [(dev, (dev + 1) % 8) for dev in range(8)])]
    reduce_sum x3, other arithmetic: 2.82 us -> 0.57 us  [row_norm(): jnp.mean(value_entries * value_entries, axis=-1, keepdims=True) + epsilon]
    unnamed x21 -> x37, local copies, waits for them, and re-layouts: 4.98 us -> 5.07 us
  transfers between devices with their start and end apart: 5 -> 11, of which waited for: 4 -> 10; matrix products, arithmetic and copies ran while one was open for 14% -> 11% of each run, Pallas kernels for 0% -> 0%
where the time goes in v1:
time: 138 us; the launch traced here: 137 us
  waiting for transfers between devices  88.3 us (64%)
  between operations  14.4 us (10%)
  starting transfers between devices  13.4 us (10%)
  other arithmetic  8.25 us (6%)
  local copies, waits for them, and re-layouts  7.6 us (6%)
  matrix products  5.21 us (4%)
    ppermute x7, waiting for transfers between devices, shards(): lax.ppermute(ring[-1], 'sp', [(dev, (dev + 1) % 8) for dev in range(8)])  53.7 us
    all_gather x1, waiting for transfers between devices, shards(): lax.all_gather(full_depth, 'tp', axis=2, tiled=True)  26.7 us
    all_to_all x1, waiting for transfers between devices, shards(): lax.all_to_all(key_slots, 'tp', split_axis=1, concat_axis=0, tiled=True)  6.25 us
    another operation x2, other arithmetic  5.17 us
    unnamed x37, local copies, waits for them, and re-layouts  5.07 us
    dot_general x1, matrix products, shards(): jnp.einsum('rd,kdc->krc', normed, lax.all_gather(full_depth, 'tp', axis=2...  4.62 us
    all_to_all x1, starting transfers between devices, shards(): lax.all_to_all(key_slots, 'tp', split_axis=1, concat_axis=0, tiled=True)  3.59 us
    all_to_all x1, starting transfers between devices, shards(): lax.all_to_all(value_slots, 'tp', split_axis=1, concat_axis=0, tiled=True)  3.46 us
  transfers between devices with their start and end apart: 11, of which 10 were waited for; matrix products, arithmetic and copies ran while one was open for 11% of the time, Pallas kernels for 0%

profile of v1, /device:TPU:0, one launch (start us, length us, event | category | flops | bytes accessed | tf_op | source)
XLA Modules:
  0.0 137.1 jit_solution(12285355865215490339)
XLA Ops:
  7.2 0.9 copy.25
  8.2 0.9 copy.26
  9.1 3.0 %collective-permute-start = (bf16[2,256,128]{1,2,0:T(8,128)(2,1)S(1)}, bf16[2,256,128]{1,2,0:T(8,128)(2,1)S(1)}, u32[]{:S(2)}, u32[]{:S(2)}) collective-permute-start(bf16[2,256,128]{1,2,0:T(8,128)(2,1)S(1)} %pad_maximum_fusion), channel_id=1, source_target_pairs={{0,4},{4,8},{8,12},{12,16},{16,20},{20,24},{24,28},{28,0},{1,5},{5... | collective-permute-start | bytes 393224 | tf_op jit(solution)/shard_map/ppermute | solution.py:38
  12.1 6.5 %collective-permute-done = bf16[2,256,128]{1,2,0:T(8,128)(2,1)S(1)} collective-permute-done((bf16[2,256,128]{1,2,0:T(8,128)(2,1)S(1)}, bf16[2,256,128]{1,2,0:T(8,128)(2,1)S(1)}, u32[]{:S(2)}, u32[]{:S(2)}) %collective-permute-start) | collective-permute-done | bytes 131104 | tf_op jit(solution)/shard_map/ppermute | solution.py:38
  18.7 7.7 %collective-permute-done.1 = bf16[2,256,128]{1,2,0:T(8,128)(2,1)S(1)} collective-permute-done((bf16[2,256,128]{1,2,0:T(8,128)(2,1)S(1)}, bf16[2,256,128]{1,2,0:T(8,128)(2,1)S(1)}, u32[]{:S(2)}, u32[]{:S(2)}) %collective-permute-start.1) | collective-permute-done | bytes 131104 | tf_op jit(solution)/shard_map/ppermute | solution.py:38
  26.3 7.7 %collective-permute-done.2 = bf16[2,256,128]{1,2,0:T(8,128)(2,1)S(1)} collective-permute-done((bf16[2,256,128]{1,2,0:T(8,128)(2,1)S(1)}, bf16[2,256,128]{1,2,0:T(8,128)(2,1)S(1)}, u32[]{:S(2)}, u32[]{:S(2)}) %collective-permute-start.2) | collective-permute-done | bytes 131104 | tf_op jit(solution)/shard_map/ppermute | solution.py:38
  34.0 7.7 %collective-permute-done.3 = bf16[2,256,128]{1,2,0:T(8,128)(2,1)S(1)} collective-permute-done((bf16[2,256,128]{1,2,0:T(8,128)(2,1)S(1)}, bf16[2,256,128]{1,2,0:T(8,128)(2,1)S(1)}, u32[]{:S(2)}, u32[]{:S(2)}) %collective-permute-start.3) | collective-permute-done | bytes 131104 | tf_op jit(solution)/shard_map/ppermute | solution.py:38
  41.7 7.7 %collective-permute-done.4 = bf16[2,256,128]{1,2,0:T(8,128)(2,1)S(1)} collective-permute-done((bf16[2,256,128]{1,2,0:T(8,128)(2,1)S(1)}, bf16[2,256,128]{1,2,0:T(8,128)(2,1)S(1)}, u32[]{:S(2)}, u32[]{:S(2)}) %collective-permute-start.4) | collective-permute-done | bytes 131104 | tf_op jit(solution)/shard_map/ppermute | solution.py:38
  49.4 8.9 %collective-permute-done.5 = bf16[2,256,128]{1,2,0:T(8,128)(2,1)S(1)} collective-permute-done((bf16[2,256,128]{1,2,0:T(8,128)(2,1)S(1)}, bf16[2,256,128]{1,2,0:T(8,128)(2,1)S(1)}, u32[]{:S(2)}, u32[]{:S(2)}) %collective-permute-start.5) | collective-permute-done | bytes 131104 | tf_op jit(solution)/shard_map/ppermute | solution.py:38
  58.2 7.7 %collective-permute-done.6 = bf16[2,256,128]{1,2,0:T(8,128)(2,1)S(1)} collective-permute-done((bf16[2,256,128]{1,2,0:T(8,128)(2,1)S(1)}, bf16[2,256,128]{1,2,0:T(8,128)(2,1)S(1)}, u32[]{:S(2)}, u32[]{:S(2)}) %collective-permute-start.6) | collective-permute-done | bytes 131104 | tf_op jit(solution)/shard_map/ppermute | solution.py:38
  66.2 1.1 constant_dynamic-slice_fusion
  68.5 0.7 reshape.96
  69.2 3.3 %all-to-all-start.2 = ((bf16[4,2,192]{2,1,0:T(2,128)(2,1)}), bf16[4,2,192]{2,1,0:T(2,128)(2,1)S(1)}, u32[]{:S(2)}, u32[]{:S(2)}) async-start(bf16[4,2,192]{2,1,0:T(2,128)(2,1)} %reshape.96), calls=%async_computation.2 | async-start | bytes 8192 | tf_op jit(solution)/shard_map/all_to_all | solution.py:59
  73.0 26.7 %all-gather.2.cloned.1.call-done = bf16[2,2048,512]{1,2,0:T(8,128)(2,1)} async-done(((bf16[2,2048,128]{1,2,0:T(8,128)(2,1)}), bf16[2,2048,512]{1,2,0:T(8,128)(2,1)}) %all-gather.2.cloned.1.call-update) | async-done | bytes 4194320 | tf_op jit(solution)/shard_map/all_gather | solution.py:45
  99.7 4.6 %fusion.10 = f32[2,384,512]{1,2,0:T(8,128)S(1)} fusion(bf16[2,2048,512]{1,2,0:T(8,128)(2,1)} %all-gather.2.cloned.1.call-done, bf16[1,384,2048]{2,1,0:T(8,128)(2,1)S(1)} %copy-done, f32[2048]{0:T(1024)S(1)} %copy-done.7, f32[384]{0:T(512)S(1)} %add_rsqrt_fusion.1), kind=kOutput, calls=%fused_computation.12 | convolution fusion | flops 1613758464 | bytes 7349760 | tf_op jit(solution)/shard_map/rd,kdc->krc/dot_general | solution.py:42
  104.9 1.0 multiply_convert_fusion
  106.0 3.6 %all-to-all-start = ((bf16[384,4,128]{2,0,1:T(8,128)(2,1)}), bf16[384,4,128]{2,0,1:T(8,128)(2,1)S(1)}, u32[]{:S(2)}, u32[]{:S(2)}) async-start(bf16[384,4,128]{2,0,1:T(8,128)(2,1)} %multiply_convert_fusion), calls=%async_computation | async-start | bytes 786432 | tf_op jit(solution)/shard_map/all_to_all | solution.py:57
  109.8 0.9 copy.28
  110.7 6.3 %all-to-all-done = bf16[384,4,128]{2,0,1:T(8,128)(2,1)S(1)} async-done(((bf16[384,4,128]{2,0,1:T(8,128)(2,1)}), bf16[384,4,128]{2,0,1:T(8,128)(2,1)S(1)}, u32[]{:S(2)}, u32[]{:S(2)}) %all-to-all-start) | async-done | bytes 393248 | tf_op jit(solution)/shard_map/all_to_all | solution.py:57
  116.9 3.5 %all-to-all-start.1 = ((bf16[384,4,128]{2,0,1:T(8,128)(2,1)}), bf16[384,4,128]{2,0,1:T(8,128)(2,1)S(1)}, u32[]{:S(2)}, u32[]{:S(2)}) async-start(bf16[384,4,128]{2,0,1:T(8,128)(2,1)} %copy.28), calls=%async_computation.1 | async-start | bytes 786432 | tf_op jit(solution)/shard_map/all_to_all | solution.py:58
  120.7 5.0 %reduce-window.6 = f32[4,12,128]{2,1,0:T(8,128)S(1)} reduce-window(f32[4,12,128]{2,1,0:T(8,128)S(1)} %reshape.89, f32[]{:T(128)} %constant.50.clone.1), window={size=1x1x128 pad=0_0x0_0x0_127}, to_apply=%region_3.4 | reduce-window | flops 780288 | bytes 49156 | tf_op jit(solution)/shard_map/reduce-window
  126.1 1.7 %all-to-all-done.1 = bf16[384,4,128]{2,0,1:T(8,128)(2,1)S(1)} async-done(((bf16[384,4,128]{2,0,1:T(8,128)(2,1)}), bf16[384,4,128]{2,0,1:T(8,128)(2,1)S(1)}, u32[]{:S(2)}, u32[]{:S(2)}) %all-to-all-start.1) | async-done | bytes 393248 | tf_op jit(solution)/shard_map/all_to_all | solution.py:58
  128.8 0.7 copy.54
  129.5 0.7 copy.55
  (66 shorter events, 4.5 us)
Async XLA Ops:
  7.2 92.5 %all-gather.2.cloned.1.call-start = ((), (), s32[]{:S(2)}) async-start(), calls=%async_computation.3 | async-start | bytes 5242880 | tf_op jit(solution)/shard_map/all_gather | solution.py:45
  9.1 9.6 %collective-permute-start = (bf16[2,256,128]{1,2,0:T(8,128)(2,1)S(1)}, bf16[2,256,128]{1,2,0:T(8,128)(2,1)S(1)}, u32[]{:S(2)}, u32[]{:S(2)}) collective-permute-start(bf16[2,256,128]{1,2,0:T(8,128)(2,1)S(1)} %pad_maximum_fusion), channel_id=1, source_target_pairs={{0,4},{4,8},{8,12},{12,16},{16,20},{20,24},{24,28},{28,0},{1,5},{5... | collective-permute-start | bytes 393224 | tf_op jit(solution)/shard_map/ppermute | solution.py:38
  18.7 7.7 %collective-permute-start.1 = (bf16[2,256,128]{1,2,0:T(8,128)(2,1)S(1)}, bf16[2,256,128]{1,2,0:T(8,128)(2,1)S(1)}, u32[]{:S(2)}, u32[]{:S(2)}) collective-permute-start(bf16[2,256,128]{1,2,0:T(8,128)(2,1)S(1)} %collective-permute-done), channel_id=1, source_target_pairs={{0,4},{4,8},{8,12},{12,16},{16,20},{20,24},{24,28},{28,0},{1,5},{5... | collective-permute-start | bytes 393224 | tf_op jit(solution)/shard_map/ppermute | solution.py:38
  26.3 7.7 %collective-permute-start.2 = (bf16[2,256,128]{1,2,0:T(8,128)(2,1)S(1)}, bf16[2,256,128]{1,2,0:T(8,128)(2,1)S(1)}, u32[]{:S(2)}, u32[]{:S(2)}) collective-permute-start(bf16[2,256,128]{1,2,0:T(8,128)(2,1)S(1)} %collective-permute-done.1), channel_id=1, source_target_pairs={{0,4},{4,8},{8,12},{12,16},{16,20},{20,24},{24,28},{28,0},{1,5},{5... | collective-permute-start | bytes 393224 | tf_op jit(solution)/shard_map/ppermute | solution.py:38
  34.0 7.7 %collective-permute-start.3 = (bf16[2,256,128]{1,2,0:T(8,128)(2,1)S(1)}, bf16[2,256,128]{1,2,0:T(8,128)(2,1)S(1)}, u32[]{:S(2)}, u32[]{:S(2)}) collective-permute-start(bf16[2,256,128]{1,2,0:T(8,128)(2,1)S(1)} %collective-permute-done.2), channel_id=1, source_target_pairs={{0,4},{4,8},{8,12},{12,16},{16,20},{20,24},{24,28},{28,0},{1,5},{5... | collective-permute-start | bytes 393224 | tf_op jit(solution)/shard_map/ppermute | solution.py:38
  41.7 7.7 %collective-permute-start.4 = (bf16[2,256,128]{1,2,0:T(8,128)(2,1)S(1)}, bf16[2,256,128]{1,2,0:T(8,128)(2,1)S(1)}, u32[]{:S(2)}, u32[]{:S(2)}) collective-permute-start(bf16[2,256,128]{1,2,0:T(8,128)(2,1)S(1)} %collective-permute-done.3), channel_id=1, source_target_pairs={{0,4},{4,8},{8,12},{12,16},{16,20},{20,24},{24,28},{28,0},{1,5},{5... | collective-permute-start | bytes 393224 | tf_op jit(solution)/shard_map/ppermute | solution.py:38
  49.4 8.9 %collective-permute-start.5 = (bf16[2,256,128]{1,2,0:T(8,128)(2,1)S(1)}, bf16[2,256,128]{1,2,0:T(8,128)(2,1)S(1)}, u32[]{:S(2)}, u32[]{:S(2)}) collective-permute-start(bf16[2,256,128]{1,2,0:T(8,128)(2,1)S(1)} %collective-permute-done.4), channel_id=1, source_target_pairs={{0,4},{4,8},{8,12},{12,16},{16,20},{20,24},{24,28},{28,0},{1,5},{5... | collective-permute-start | bytes 393224 | tf_op jit(solution)/shard_map/ppermute | solution.py:38
  58.2 7.7 %collective-permute-start.6 = (bf16[2,256,128]{1,2,0:T(8,128)(2,1)S(1)}, bf16[2,256,128]{1,2,0:T(8,128)(2,1)S(1)}, u32[]{:S(2)}, u32[]{:S(2)}) collective-permute-start(bf16[2,256,128]{1,2,0:T(8,128)(2,1)S(1)} %collective-permute-done.5), channel_id=1, source_target_pairs={{0,4},{4,8},{8,12},{12,16},{16,20},{20,24},{24,28},{28,0},{1,5},{5... | collective-permute-start | bytes 393224 | tf_op jit(solution)/shard_map/ppermute | solution.py:38
  66.1 1.2 copy-start.2
  66.1 6.3 %copy-start.3 = (bf16[1,4,128]{2,1,0:T(4,128)(2,1)S(1)}, bf16[1,4,128]{2,1,0:T(4,128)(2,1)}, u32[]{:S(2)}) copy-start(bf16[1,4,128]{2,1,0:T(4,128)(2,1)} %param.15) | copy-start | bytes 3076
  66.2 6.5 %copy-start = (bf16[1,384,2048]{2,1,0:T(8,128)(2,1)S(1)}, bf16[1,384,2048]{2,1,0:T(8,128)(2,1)}, u32[]{:S(2)}) copy-start(bf16[1,384,2048]{2,1,0:T(8,128)(2,1)} %param.9) | copy-start | bytes 4718596
  66.2 33.4 %copy-start.7 = (f32[2048]{0:T(1024)S(1)}, f32[2048]{0:T(1024)}, u32[]{:S(2)}) copy-start(f32[2048]{0:T(1024)} %param.10) | copy-start | bytes 24580
  69.2 36.7 %all-to-all-start.2 = ((bf16[4,2,192]{2,1,0:T(2,128)(2,1)}), bf16[4,2,192]{2,1,0:T(2,128)(2,1)S(1)}, u32[]{:S(2)}, u32[]{:S(2)}) async-start(bf16[4,2,192]{2,1,0:T(2,128)(2,1)} %reshape.96), calls=%async_computation.2 | async-start | bytes 8192 | tf_op jit(solution)/shard_map/all_to_all | solution.py:59
  104.3 0.7 copy-start.4
  104.9 15.5 %copy-start.5 = (f32[128]{0:T(128)S(1)}, f32[128]{0:T(128)}, u32[]{:S(2)}) copy-start(f32[128]{0:T(128)} %param.16) | copy-start | bytes 1540
  106.0 22.2 %copy-start.6 = (f32[128]{0:T(128)S(1)}, f32[128]{0:T(128)}, u32[]{:S(2)}) copy-start(f32[128]{0:T(128)} %param.17) | copy-start | bytes 1540
  106.0 11.0 %all-to-all-start = ((bf16[384,4,128]{2,0,1:T(8,128)(2,1)}), bf16[384,4,128]{2,0,1:T(8,128)(2,1)S(1)}, u32[]{:S(2)}, u32[]{:S(2)}) async-start(bf16[384,4,128]{2,0,1:T(8,128)(2,1)} %multiply_convert_fusion), calls=%async_computation | async-start | bytes 786432 | tf_op jit(solution)/shard_map/all_to_all | solution.py:57
  109.7 19.8 %copy-start.1 = (bf16[4,1,384]{2,1,0:T(2,128)(2,1)}, bf16[4,1,384]{2,1,0:T(2,128)(2,1)S(1)}, u32[]{:S(2)}) copy-start(bf16[4,1,384]{2,1,0:T(2,128)(2,1)S(1)} %reshape.97) | copy-start | bytes 9220
  116.9 10.8 %all-to-all-start.1 = ((bf16[384,4,128]{2,0,1:T(8,128)(2,1)}), bf16[384,4,128]{2,0,1:T(8,128)(2,1)S(1)}, u32[]{:S(2)}, u32[]{:S(2)}) async-start(bf16[384,4,128]{2,0,1:T(8,128)(2,1)} %copy.28), calls=%async_computation.1 | async-start | bytes 786432 | tf_op jit(solution)/shard_map/all_to_all | solution.py:58
Sparse Core Ops, SparseCore 0:
  67.4 32.1 all-gather.1
